TPU v7x, 32 devices: a whole 2x2x4 slice. The times are simulated.
32 devices in a mesh: ep: 8 (over z, x), tp: 4 (over y, core).
Axes of the slice: x: 2, y: 2, z: 4, core: 2. Of those that a mesh axis runs over, the one named last changes fastest.
Arguments:
- mix_bgate: bfloat16 [2048, 1024], P('ep', 'tp'), may hold values from -6 to 6
- mix_cgate: bfloat16 [2048, 1024], P('ep', 'tp'), may hold values from -6 to 6
- mix_input: bfloat16 [2048, 1024], P('ep', 'tp'), may hold values from -6 to 6
- conv_taps: float32 [3, 1024], P(None, 'tp'), may hold values from -3.5 to 3.5
- mix_out_w: bfloat16 [1024, 2048], P('tp'), may hold values from -0.1875 to 0.1875
- moe_x: bfloat16 [2048, 2048], P('ep', 'tp'), may hold values from -6 to 6
- moe_gain: float32 [2048], replicated, may hold values from 0.1 to 1.9
- routes: int32 [2048, 2], P('ep'), may hold values from 0 to 7, all different within a row; in each aligned block of 256 rows (0 to 255, 256 to 511, ...) at most 96 rows name the same one
- route_w: float32 [2048, 2], P('ep'), may hold values from 0.2 to 1
- w_gate: bfloat16 [8, 2048, 3584], P('ep', None, 'tp'), may hold values from -0.125 to 0.125
- w_up: bfloat16 [8, 2048, 3584], P('ep', None, 'tp'), may hold values from -0.125 to 0.125
- w_down: bfloat16 [8, 3584, 2048], P('ep', 'tp'), may hold values from -0.09375 to 0.09375
Outputs:
- mixed: bfloat16 [2048, 2048], P(('ep', 'tp'))
- routed: bfloat16 [2048, 2048], P('ep', 'tp')
Inputs may be any that keep to these rules, and one draw needn't show every extreme that they name: `routes`: among the 256 rows of one index of ep, each row names 2 different experts and no expert is named by more than 96 rows; in every draw some expert is named by exactly 96 rows of some index.
All inputs are finite; a program needn't handle non-finite values.
Results may differ from a plain program's by a relative error of at most 0.012.
Values may be sent and summed in bfloat16 or wider, within the bound.
A program may use at most 64 MiB of HBM per device.

v0:
```python
import functools

import jax
import jax.numpy as jnp
from jax import lax
from jax.experimental import pallas as pl
from jax.experimental.pallas import tpu as pltpu
from jax.sharding import PartitionSpec as P

BF16 = jnp.bfloat16
F32 = jnp.float32
MESH = pl.DeviceIdType.MESH


def flip(index, bits):
    bit = 1
    while bit <= bits:
        if bits & bit:
            index = index + bit - 2 * bit * ((index // bit) % 2)
        bit *= 2
    return index


def split_terms(value):
    high = value.astype(BF16)
    return high, (value - high.astype(F32)).astype(BF16)


def dot(a, b):
    return jnp.dot(a, b, preferred_element_type=F32)


def sizes_of(ntok, top, experts):
    cap = 4 * ((3 * ntok * top + 8 * experts - 1) // (8 * experts))
    return -(-cap // 16) * 16


def kernel(
    n_ep,
    n_tp,
    cap,
    per_group,
    bgate,
    cgate,
    inputs,
    taps,
    out_w,
    x,
    gain,
    routes,
    routes_t,
    route_w,
    w_gate,
    w_up,
    w_down,
    mixed,
    routed,
    wgu,
    wd,
    wo,
    halo,
    prod,
    gated,
    share,
    share_in,
    share_sum,
    share_far,
    squares,
    sent,
    rows,
    hidden,
    part,
    part_in,
    part_sum,
    part_far,
    final,
    back,
    at_high,
    at_low,
    total,
    gate_sem,
    up_sem,
    plain_sem,
    halo_sem,
    square_sem,
    share_sem,
    go_sem,
    far_sem,
    near_sem,
    near2_sem,
    part_sem,
    part_far_sem,
    back_sem,
):
    ep = lax.axis_index("ep")
    tp = lax.axis_index("tp")
    ntok, d = x.shape
    length, chans = cgate.shape
    reach = taps.shape[0] - 1
    d_all = n_tp * d
    ff = w_down.shape[1]
    groups = n_ep // per_group
    grows = per_group * cap
    near = flip(tp, 1)
    far = flip(tp, 2)
    cross = flip(tp, 3)
    mine = pl.ds(pl.multiple_of(tp * d, 128), d)
    theirs = pl.ds(pl.multiple_of(far * d, 128), d)
    next_ep = (ep + 1) % n_ep

    tiles = ff // 128
    loads = []
    for i in range(tiles):
        for src, sem, at in ((w_gate, gate_sem, 0), (w_up, up_sem, 128)):
            copy = pltpu.make_async_copy(
                src.at[0, :, pl.ds(i * 128, 128)], wgu.at[:, pl.ds(i * 256 + at, 128)], sem.at[i]
            )
            copy.start()
            loads.append(copy)
    down_load = pltpu.make_async_copy(w_down.at[0], wd, plain_sem.at[0])
    down_load.start()
    loads.append(down_load)
    out_load = pltpu.make_async_copy(out_w, wo, plain_sem.at[1])
    out_load.start()

    barrier = pltpu.get_barrier_semaphore()
    for j in range(1, n_ep):
        pl.semaphore_signal(barrier, inc=1, device_id=(flip(ep, j), tp), device_id_type=MESH)
    for t in (near, far, cross):
        pl.semaphore_signal(barrier, inc=1, device_id=(ep, t), device_id_type=MESH)

    def slots_by_lane():
        e_iota = lax.broadcasted_iota(jnp.int32, (n_ep, ntok), 0)
        chosen = [routes_t[k : k + 1, :] == e_iota for k in range(2)]
        named = jnp.where(chosen[0] | chosen[1], 1.0, 0.0).astype(BF16)
        row = lax.broadcasted_iota(jnp.int32, (ntok, ntok), 0)
        col = lax.broadcasted_iota(jnp.int32, (ntok, ntok), 1)
        rank = dot(named, jnp.where(row < col, 1.0, 0.0).astype(BF16))
        slot = rank + (e_iota * cap).astype(F32)
        return [jnp.sum(jnp.where(c, slot, 0.0), axis=0, keepdims=True) for c in chosen]

    lane_slots = slots_by_lane()
    wide = x[...].astype(F32)
    ones = jnp.ones((8, d), BF16)
    own_squares = jnp.zeros((8, ntok), F32)
    for term in split_terms(wide * wide):
        own_squares = own_squares + lax.dot_general(
            ones, term, (((1,), (1,)), ((), ())), preferred_element_type=F32
        )
    squares[tp] = own_squares

    pl.semaphore_wait(barrier, n_ep + 2)

    def remote(src, dst, sems, i, device):
        return pltpu.make_async_remote_copy(
            src_ref=src,
            dst_ref=dst,
            send_sem=sems.at[0, i],
            recv_sem=sems.at[1, i],
            device_id=device,
            device_id_type=MESH,
        )

    started = []

    def send(copy):
        copy.start()
        started.append(copy)

    square_copies = [
        remote(squares.at[tp], squares.at[tp], square_sem, i, (ep, flip(tp, i + 1)))
        for i in range(3)
    ]
    for copy in square_copies:
        send(copy)
    halo_copies = [
        remote(ref.at[pl.ds(length - 16, 16)], halo.at[i], halo_sem, i, (next_ep, tp))
        for i, ref in enumerate((cgate, inputs))
    ]
    for copy in halo_copies:
        send(copy)

    for copy in square_copies:
        copy.wait_recv()
    sums = squares[0]
    for i in range(1, n_tp):
        sums = sums + squares[i]
    scale = lax.rsqrt(sums / d_all + 1e-06)[0:1, :]

    def block(i):
        return pl.ds(pl.multiple_of(i * cap, 16), cap)

    def group_rows(g):
        first = flip(ep, g * per_group) // per_group * per_group
        return first, pl.ds(pl.multiple_of(first * cap, 16), grows)

    go = [None] * n_ep
    own_gain = gain[:, mine]
    for g in range(groups):
        first, span = group_rows(g)
        at = (lax.broadcasted_iota(jnp.int32, (grows, ntok), 0) + first * cap).astype(F32)
        hit = (at == lane_slots[0]) | (at == lane_slots[1])
        high, low = split_terms(jnp.where(hit, scale, 0.0))
        picked = (dot(high, x[...]) + dot(low, x[...])) * own_gain
        sent[span] = picked.astype(BF16)
        for j in range(g * per_group, (g + 1) * per_group):
            if j == 0:
                rows[block(ep), mine] = sent[block(ep)]
            else:
                to = flip(ep, j)
                go[j] = remote(sent.at[block(to)], rows.at[block(ep), mine], go_sem, j, (to, tp))
                send(go[j])

    def hop(j, columns, sems, device):
        at = (block(flip(ep, j)), columns)
        return remote(rows.at[at], rows.at[at], sems, j, (ep, device))

    to_far = [hop(j, mine, far_sem, far) for j in range(n_ep)]
    to_near = [hop(j, mine, near_sem, near) for j in range(n_ep)]
    on_near = [hop(j, theirs, near2_sem, near) for j in range(n_ep)]

    def arrive(js):
        for j in js:
            if j:
                go[j].wait_recv()
            send(to_far[j])
            send(to_near[j])

    def relay(js):
        for j in js:
            to_far[j].wait_recv()
            send(on_near[j])

    def ready(js):
        for j in js:
            to_near[j].wait_recv()
            on_near[j].wait_recv()

    order = (cross, near, far, tp)

    part_copies = [[None, None] for _ in range(groups)]
    part_far_copies = [None] * groups
    back_copies = [None] * n_ep

    def compute(g):
        _, span = group_rows(g)

        def tile(i, carry):
            both = dot(rows[span, :], wgu[:, pl.ds(pl.multiple_of(i * 256, 256), 256)])
            gate, upper = both[:, :128], both[:, 128:]
            act = gate / (1.0 + jnp.exp(-gate)) * upper
            hidden[:, pl.ds(pl.multiple_of(i * 128, 128), 128)] = act.astype(BF16)
            return carry

        lax.fori_loop(0, tiles, tile, 0)
        for k, p in enumerate(order):
            columns = pl.ds(pl.multiple_of(p * d, 128), d)
            part[g, k] = dot(hidden[...], wd[:, columns]).astype(BF16)
            if k < 2:
                part_copies[g][k] = remote(
                    part.at[g, k], part_in.at[g, k], part_sem, 2 * g + k, (ep, near)
                )
                send(part_copies[g][k])

    def add_near(g):
        part_copies[g][0].wait_recv()
        part_sum[g] = (part[g, 2].astype(F32) + part_in[g, 0].astype(F32)).astype(BF16)
        part_far_copies[g] = remote(
            part_sum.at[g], part_far.at[g], part_far_sem, g, (ep, far)
        )
        send(part_far_copies[g])

    def add_far(g):
        first, span = group_rows(g)
        part_copies[g][1].wait_recv()
        near_sum = part[g, 3].astype(F32) + part_in[g, 1].astype(F32)
        part_far_copies[g].wait_recv()
        final[span] = (near_sum + part_far[g].astype(F32)).astype(BF16)
        for j in range(g * per_group, (g + 1) * per_group):
            if j == 0:
                back[block(ep)] = final[block(ep)]
            else:
                to = flip(ep, j)
                back_copies[j] = remote(
                    final.at[block(to)], back.at[block(ep)], back_sem, j, (to, tp)
                )
                send(back_copies[j])

    def collect(g):
        _, span = group_rows(g)
        for j in range(g * per_group, (g + 1) * per_group):
            if j:
                back_copies[j].wait_recv()
        got = back[span]
        now = dot(at_high[g], got) + dot(at_low[g], got)
        if g == 0:
            total[...] = now
        elif g < groups - 1:
            total[...] += now
        else:
            routed[...] = (total[...] + now).astype(BF16)

    part_rows = length // n_tp

    def part_of(p):
        return pl.ds(pl.multiple_of(p * part_rows, 16), part_rows)

    share_copies = []

    def mix():
        for copy in halo_copies:
            copy.wait_recv()
        before = halo[0].astype(F32) * halo[1].astype(F32)
        prod[0:16, :] = jnp.where(ep > 0, before, 0.0)
        prod[16:, :] = cgate[...].astype(F32) * inputs[...].astype(F32)
        conv = taps[0:1, :] * prod[16 - reach : 16 - reach + length, :]
        for j in range(1, reach + 1):
            conv = conv + taps[j : j + 1, :] * prod[16 - reach + j : 16 - reach + j + length, :]
        gated[...] = (bgate[...].astype(F32) * conv).astype(BF16)
        out_load.wait()

        def tile(i, carry):
            columns = pl.ds(pl.multiple_of(i * 256, 256), 256)
            share[:, columns] = dot(gated[...], wo[:, columns]).astype(BF16)
            return carry

        lax.fori_loop(0, d_all // 256, tile, 0)
        for k in range(2):
            share_copies.append(
                remote(share.at[part_of(order[k])], share_in.at[k], share_sem, k, (ep, near))
            )
            send(share_copies[k])

    def mix_near():
        share_copies[0].wait_recv()
        share_sum[...] = (
            share[part_of(far), :].astype(F32) + share_in[0].astype(F32)
        ).astype(BF16)
        share_copies.append(remote(share_sum, share_far, share_sem, 2, (ep, far)))
        send(share_copies[2])

    def mix_far():
        share_copies[1].wait_recv()
        near_sum = share[part_of(tp), :].astype(F32) + share_in[1].astype(F32)
        share_copies[2].wait_recv()
        mixed[...] = (near_sum + share_far[...].astype(F32)).astype(BF16)

    def tables():
        e_iota = lax.broadcasted_iota(jnp.int32, (ntok, n_ep), 1)
        chosen = [routes[:, k : k + 1] == e_iota for k in range(2)]
        named = jnp.where(chosen[0] | chosen[1], 1.0, 0.0).astype(BF16)
        row = lax.broadcasted_iota(jnp.int32, (ntok, ntok), 0)
        col = lax.broadcasted_iota(jnp.int32, (ntok, ntok), 1)
        rank = dot(jnp.where(col < row, 1.0, 0.0).astype(BF16), named)
        slot = rank + (e_iota * cap).astype(F32)
        slots = [jnp.sum(jnp.where(c, slot, 0.0), axis=1, keepdims=True) for c in chosen]
        for g in range(groups):
            first, _ = group_rows(g)
            at = (lax.broadcasted_iota(jnp.int32, (ntok, grows), 1) + first * cap).astype(F32)
            value = jnp.where(at == slots[0], route_w[:, 0:1], 0.0) + jnp.where(
                at == slots[1], route_w[:, 1:2], 0.0
            )
            at_high[g], at_low[g] = split_terms(value)

    half = per_group // 2

    def first_half(g):
        return range(g * per_group, g * per_group + half)

    def second_half(g):
        return range(g * per_group + half, (g + 1) * per_group)

    def whole(g):
        return range(g * per_group, (g + 1) * per_group)

    arrive(first_half(0))
    mix()
    arrive(second_half(0))
    mix_near()
    tables()
    arrive(whole(1))
    relay(whole(0))
    for load in loads:
        load.wait()
    for g in range(groups):
        if g + 2 < groups:
            arrive(first_half(g + 2))
        ready(whole(g))
        compute(g)
        if g + 1 < groups:
            relay(whole(g + 1))
        if g + 2 < groups:
            arrive(second_half(g + 2))
        add_near(g)
        if g:
            add_far(g - 1)
    add_far(groups - 1)
    mix_far()
    for g in range(groups):
        collect(g)
    for copy in started:
        copy.wait_send()


def body(
    mix_bgate,
    mix_cgate,
    mix_input,
    conv_taps,
    mix_out_w,
    moe_x,
    moe_gain,
    routes,
    route_w,
    w_gate,
    w_up,
    w_down,
):
    ntok, d = moe_x.shape
    length, chans = mix_input.shape
    n_ep = lax.axis_size("ep")
    n_tp = lax.axis_size("tp")
    assert w_gate.shape[0] == 1 and n_tp == 4 and routes.shape[1] == 2
    assert n_ep & (n_ep - 1) == 0
    cap = sizes_of(ntok, routes.shape[1], n_ep)
    per_group = 2
    while per_group * cap < 192 and 2 * per_group * 2 <= n_ep:
        per_group *= 2
    groups = n_ep // per_group
    grows = per_group * cap
    d_all = n_tp * d
    ff = w_down.shape[1]
    slots = n_ep * cap
    part_rows = length // n_tp
    vmem = pl.BlockSpec(memory_space=pltpu.VMEM)
    anywhere = pl.BlockSpec(memory_space=pl.ANY)
    dma = pltpu.SemaphoreType.DMA
    call = pl.pallas_call(
        functools.partial(kernel, n_ep, n_tp, cap, per_group),
        out_shape=(
            jax.ShapeDtypeStruct((part_rows, d_all), BF16),
            jax.ShapeDtypeStruct((ntok, d), BF16),
        ),
        in_specs=[vmem] * 4 + [anywhere] + [vmem] * 5 + [anywhere] * 3,
        out_specs=(vmem, vmem),
        scratch_shapes=[
            pltpu.VMEM((d_all, 2 * ff), BF16),
            pltpu.VMEM((ff, d_all), BF16),
            pltpu.VMEM((chans, d_all), BF16),
            pltpu.VMEM((2, 16, chans), BF16),
            pltpu.VMEM((16 + length, chans), F32),
            pltpu.VMEM((length, chans), BF16),
            pltpu.VMEM((length, d_all), BF16),
            pltpu.VMEM((2, part_rows, d_all), BF16),
            pltpu.VMEM((part_rows, d_all), BF16),
            pltpu.VMEM((part_rows, d_all), BF16),
            pltpu.VMEM((n_tp, 8, ntok), F32),
            pltpu.VMEM((slots, d), BF16),
            pltpu.VMEM((slots, d_all), BF16),
            pltpu.VMEM((grows, ff), BF16),
            pltpu.VMEM((groups, 4, grows, d), BF16),
            pltpu.VMEM((groups, 2, grows, d), BF16),
            pltpu.VMEM((groups, grows, d), BF16),
            pltpu.VMEM((groups, grows, d), BF16),
            pltpu.VMEM((slots, d), BF16),
            pltpu.VMEM((slots, d), BF16),
            pltpu.VMEM((groups, ntok, grows), BF16),
            pltpu.VMEM((groups, ntok, grows), BF16),
            pltpu.VMEM((ntok, d), F32),
            dma((ff // 128,)),
            dma((ff // 128,)),
            dma((2,)),
            dma((2, 2)),
            dma((2, 3)),
            dma((2, 3)),
            dma((2, n_ep)),
            dma((2, n_ep)),
            dma((2, n_ep)),
            dma((2, n_ep)),
            dma((2, 2 * groups)),
            dma((2, groups)),
            dma((2, n_ep)),
        ],
        compiler_params=pltpu.CompilerParams(
            collective_id=0, has_side_effects=True, vmem_limit_bytes=56 << 20
        ),
        name="step",
    )
    return call(
        mix_bgate,
        mix_cgate,
        mix_input,
        conv_taps,
        mix_out_w,
        moe_x,
        moe_gain.reshape(1, d_all),
        routes,
        routes.T,
        route_w,
        w_gate,
        w_up,
        w_down,
    )


def solution(mesh):
    in_specs = (
        P("ep", "tp"),
        P("ep", "tp"),
        P("ep", "tp"),
        P(None, "tp"),
        P("tp", None),
        P("ep", "tp"),
        P(),
        P("ep", None),
        P("ep", None),
        P("ep", None, "tp"),
        P("ep", None, "tp"),
        P("ep", "tp", None),
    )
    out_specs = (P(("ep", "tp"), None), P("ep", "tp"))
    return jax.shard_map(body, mesh=mesh, in_specs=in_specs, out_specs=out_specs, check_vma=False)
```

profile of v0, /device:TPU:21, one launch (start us, length us, event | category | flops | bytes accessed | tf_op | source)
XLA Modules:
  0.0 76.0 jit_solution(3530564898087909439)
XLA Ops:
  0.6 1.5 %copy.15.route_w = f32[256,2]{1,0:T(8,128)} copy(f32[256,2]{0,1:T(2,128)} %param.20) | data formatting | bytes 4096 | tf_op args[8]
  2.1 1.5 %copy.14.routes = s32[256,2]{1,0:T(8,128)} copy(s32[256,2]{0,1:T(2,128)} %param.19) | data formatting | bytes 4096 | tf_op args[7]
  3.6 69.0 %step.1 = (bf16[64,2048]{1,0:T(8,128)(2,1)}, bf16[256,512]{1,0:T(8,128)(2,1)}) custom-call(bf16[256,256]{1,0:T(8,128)(2,1)} %bgate.1, bf16[256,256]{1,0:T(8,128)(2,1)} %cgate.1, bf16[256,256]{1,0:T(8,128)(2,1)} %inputs.1, f32[3,256]{1,0:T(4,128)} %taps.1, bf16[256,2048]{1,0:T(8,128)(2,1)} %out_w.1, bf16[256,512]{1,0:T(8,128)(2,1)} %x.1, f32[1,2048]{1,0:T(1,128)} %bitcast.3, ...), custom_call_target="tpu_custom_call" | custom-call | tf_op jit(solution)/shard_map/step/pallas_call | solution.py:489
  72.6 1.7 %copy.18 = bf16[64,2048]{1,0:T(8,128)(2,1)} copy(bf16[64,2048]{1,0:T(8,128)(2,1)} %get-tuple-element.4) | data formatting | bytes 524288
  74.3 1.7 %copy.19 = bf16[256,512]{1,0:T(8,128)(2,1)} copy(bf16[256,512]{1,0:T(8,128)(2,1)} %get-tuple-element.5) | data formatting | bytes 524288
where the time goes:
time: 76.2 us; the launch traced here: 76 us
  Pallas kernels  69 us (91%)
  local copies, waits for them, and re-layouts  6.29 us (8%)
    pallas_call x1, Pallas kernels, body(): call(mix_bgate, mix_cgate, mix_input, conv_taps, mix_out_w, moe_x, moe_ga...  69 us
    unnamed x4, local copies, waits for them, and re-layouts  6.29 us

commit v1 on v0

v1 whole, which is shorter than its diff:
```python
import functools

import jax
import jax.numpy as jnp
from jax import lax
from jax.experimental import pallas as pl
from jax.experimental.pallas import tpu as pltpu
from jax.sharding import PartitionSpec as P

BF16 = jnp.bfloat16
F32 = jnp.float32
MESH = pl.DeviceIdType.MESH
scope = jax.named_scope

PLAN = (
    "D4", "D6", "D1", "D2", "D3", "A0", "S", "X", "T", "A1", "Q", "A4", "P", "G2", "G1", "D5",
    "G3", "D7", "B0", "Y0", "A2", "R4", "A6", "Y1", "L", "C4", "A3", "B2", "O4", "R6", "C0",
    "N4", "A5", "O0", "Y2", "B1", "B3", "C6", "F4", "O6", "A7", "N0", "N6", "C1", "R5", "O1",
    "Y3", "N1", "C5", "F6", "R7", "O5", "H0", "N5", "C7", "H1", "O7", "M0", "N7", "F5", "M1",
    "W", "F7", "Z", "K4", "K0", "K6", "K1", "K5", "K7", "E",
)


def flip(index, bits):
    bit = 1
    while bit <= bits:
        if bits & bit:
            index = index + bit - 2 * bit * ((index // bit) % 2)
        bit *= 2
    return index


def split_terms(value):
    high = value.astype(BF16)
    return high, (value - high.astype(F32)).astype(BF16)


def dot(a, b):
    return jnp.dot(a, b, preferred_element_type=F32)


def sizes_of(ntok, top, experts):
    cap = 4 * ((3 * ntok * top + 8 * experts - 1) // (8 * experts))
    return -(-cap // 16) * 16


def kernel(
    n_ep,
    n_tp,
    cap,
    bgate_in,
    cgate_in,
    inputs_in,
    taps_in,
    out_w,
    x_in,
    gain_in,
    routes_in,
    weight_in,
    w_gate,
    w_up,
    w_down,
    mixed,
    routed,
    x,
    routes_t,
    inputs,
    cgate,
    bgate,
    taps,
    weight_t,
    gain,
    wgu,
    wd,
    wo,
    halo,
    prod,
    gated,
    share,
    share_in,
    share_sum,
    share_far,
    x_far,
    sent,
    sent_far,
    rows,
    normed,
    hidden,
    part,
    part_in,
    part_sum,
    part_far,
    final,
    back,
    back_far,
    at_high,
    at_low,
    total,
    total_far,
    total_out,
    total_in,
    in_sem,
    gate_sem,
    up_sem,
    plain_sem,
    halo_sem,
    share_sem,
    cross_sem,
    go_sem,
    go_far_sem,
    far_sem,
    near_sem,
    near2_sem,
    part_sem,
    part_far_sem,
    back_sem,
    back_far_sem,
):
    ep = lax.axis_index("ep")
    tp = lax.axis_index("tp")
    ntok, d = x_in.shape
    length, chans = cgate_in.shape
    reach = taps_in.shape[0] - 1
    d_all = n_tp * d
    ff = w_down.shape[1]
    run_length = n_ep // 8
    near = flip(tp, 1)
    far = flip(tp, 2)
    cross = flip(tp, 3)
    mine = pl.ds(pl.multiple_of(tp * d, 128), d)
    theirs = pl.ds(pl.multiple_of(far * d, 128), d)
    next_ep = (ep + 1) % n_ep

    barrier = pltpu.get_barrier_semaphore()
    for j in range(1, n_ep):
        pl.semaphore_signal(barrier, inc=1, device_id=(flip(ep, j), tp), device_id_type=MESH)
    for t in (near, far):
        pl.semaphore_signal(barrier, inc=1, device_id=(ep, t), device_id_type=MESH)

    def load(i, source, dest):
        copy = pltpu.make_async_copy(source, dest, in_sem.at[i])
        copy.start()
        return copy

    first_loads = [load(0, routes_in, routes_t), load(1, x_in, x)]
    mix_loads = [
        load(2, inputs_in, inputs),
        load(3, cgate_in, cgate),
        load(4, bgate_in, bgate),
        load(5, taps_in, taps),
        load(6, out_w, wo),
    ]
    late_loads = [load(7, weight_in, weight_t), load(8, gain_in, gain)]

    def wait_all(copies):
        for copy in copies:
            copy.wait()
        copies.clear()

    def run_of(r):
        return range(r * run_length, (r + 1) * run_length)

    def place(i):
        low, run, high = i % run_length, i // run_length % 4, i // run_length // 4
        return (4 * high + 2 * (run % 2) + run // 2) * run_length + low

    def block(i):
        return pl.ds(pl.multiple_of(place(i) * cap, 16), cap)

    half = ep // (4 * run_length) % 2
    step = ep // (2 * run_length) % 2
    inner = half + step - 2 * half * step

    def member(j):
        to = flip(ep, j)
        if j < 4 * run_length:
            return to
        wanted = half if j // (2 * run_length) % 2 else 1 - half
        return to + 2 * run_length * (wanted - to // (2 * run_length) % 2)

    def seen_as(j):
        if j < 4 * run_length:
            return j
        run, low = j // run_length, j % run_length
        return (4 + 2 * inner + run % 2) * run_length + low

    def rows_of(unit):
        count = len(unit) * run_length
        first = place(member(unit[0] * run_length)) // count * count * cap
        return first, count * cap

    def span_of(unit):
        first, count = rows_of(unit)
        return pl.ds(pl.multiple_of(first, 16), count)

    def slots_by_lane():
        e_iota = lax.broadcasted_iota(jnp.int32, (n_ep, ntok), 0)
        chosen = [routes_t[k : k + 1, :] == e_iota for k in range(2)]
        named = jnp.where(chosen[0] | chosen[1], 1.0, 0.0).astype(BF16)
        row = lax.broadcasted_iota(jnp.int32, (ntok, ntok), 0)
        col = lax.broadcasted_iota(jnp.int32, (ntok, ntok), 1)
        rank = dot(named, jnp.where(row < col, 1.0, 0.0).astype(BF16))
        slot = rank + (place(e_iota) * cap).astype(F32)
        return [jnp.sum(jnp.where(c, slot, 0.0), axis=0, keepdims=True) for c in chosen]

    wait_all(first_loads)
    lane_slots = slots_by_lane()

    sums = {0: (0, 2), 1: (1, 3), 4: (4,), 5: (5,), 6: (6,), 7: (7,)}
    units = sums
    unit_of = {u: u for u in sums}

    def slots_of(unit):
        first, count = rows_of(unit)
        return (lax.broadcasted_iota(jnp.int32, (count, ntok), 0) + first).astype(F32)

    def hits(unit):
        at = slots_of(unit)
        hit = (at == lane_slots[0]) | (at == lane_slots[1])
        return jnp.where(hit, 1.0, 0.0).astype(BF16)

    for unit in ((0, 2), (1, 3), (4, 6), (5, 7)):
        sent[span_of(unit)] = dot(hits(unit), x[...]).astype(BF16)
    rows[block(ep), mine] = sent[block(ep)]

    with scope("barrier"):
        pl.semaphore_wait(barrier, n_ep + 1)

    def remote(src, dst, sems, i, device, there=None):
        return pltpu.make_async_remote_copy(
            src_ref=src,
            dst_ref=dst,
            send_sem=sems.at[0, i],
            recv_sem=sems.at[1, i if there is None else there],
            device_id=device,
            device_id_type=MESH,
        )

    started = []

    def send(copy):
        copy.start()
        started.append(copy)

    halo_copies = [
        remote(ref.at[pl.ds(length - 16, 16)], halo.at[i], halo_sem, i, (next_ep, tp))
        for i, ref in enumerate((cgate, inputs))
    ]
    for copy in mix_loads[:2]:
        copy.wait()
    x_copy = remote(x, x_far, cross_sem, 0, (ep, far))
    for copy in halo_copies:
        send(copy)
    send(x_copy)

    def go_copy(j):
        to = flip(ep, j)
        return remote(
            sent.at[block(to)], rows.at[block(ep), mine], go_sem, j, (to, tp), seen_as(j)
        )

    def landed(dest, sems, j):
        block_of = dest.at[block(ep)] if dest is not rows else rows.at[block(ep), mine]
        remote(block_of, block_of, sems, j, (member(j), tp)).wait_recv()

    def go_far_copy(j):
        to = flip(ep, j)
        return remote(sent_far.at[block(to)], rows.at[block(ep), theirs], go_far_sem, j, (to, tp))

    go = {j: go_copy(j) for j in range(1, n_ep)}
    go_far = {j: go_far_copy(j) for j in range(1, n_ep // 2)}

    def depart(r):
        for j in run_of(r):
            if j:
                send(go[j])

    def pick_far():
        x_copy.wait_recv()
        for unit in ((0, 2), (1, 3)):
            sent_far[span_of(unit)] = dot(hits(unit), x_far[...]).astype(BF16)
        rows[block(ep), theirs] = sent_far[block(ep)]

    def depart_far(r):
        for j in run_of(r):
            if j:
                send(go_far[j])

    def hop(j, columns, sems, device):
        at = (block(member(j)), columns)
        return remote(rows.at[at], rows.at[at], sems, j, (ep, device))

    to_far = {j: hop(j, mine, far_sem, far) for j in range(n_ep // 2, n_ep)}
    to_near = [hop(j, mine, near_sem, near) for j in range(n_ep)]
    on_near = [hop(j, theirs, near2_sem, near) for j in range(n_ep)]

    def arrive(r):
        for j in run_of(r):
            if j:
                landed(rows, go_sem, j)
            if r >= 4:
                send(to_far[j])
            send(to_near[j])

    def arrive_far(r):
        for j in run_of(r):
            if j:
                go_far[j].wait_recv()
            send(on_near[j])

    def relay(r):
        for j in run_of(r):
            to_far[j].wait_recv()
            send(on_near[j])

    order = (cross, near, far, tp)

    part_copies = {}
    part_far_copies = {}

    def compute(u):
        unit = units[u]
        for r in unit:
            for j in run_of(r):
                to_near[j].wait_recv()
                on_near[j].wait_recv()
        span = span_of(unit)
        count = rows_of(unit)[1]
        wide = rows[span, :].astype(F32)
        scale = lax.rsqrt(jnp.sum(wide * wide, axis=1, keepdims=True) / d_all + 1e-06)
        normed[:count, :] = (wide * scale * gain[...]).astype(BF16)

        def tile(i, carry):
            columns = pl.ds(pl.multiple_of(i * 256, 256), 256)
            both = dot(normed[:count, :], wgu[:, columns])
            gate, upper = both[:, :128], both[:, 128:]
            act = gate / (1.0 + jnp.exp(-gate)) * upper
            hidden[:count, pl.ds(pl.multiple_of(i * 128, 128), 128)] = act.astype(BF16)
            return carry

        lax.fori_loop(0, tiles, tile, 0, unroll=True)

    def compute_down(u):
        span = span_of(units[u])
        count = rows_of(units[u])[1]
        for k, p in enumerate(order):
            columns = pl.ds(pl.multiple_of(p * d, 128), d)
            part[k, span] = dot(hidden[:count, :], wd[:, columns]).astype(BF16)
            if k < 2:
                part_copies[u, k] = remote(
                    part.at[k, span], part_in.at[k, span], part_sem, 2 * u + k, (ep, near)
                )
                send(part_copies[u, k])

    def part_wait(u, k):
        copy = part_copies.pop((unit_of[u], k), None)
        if copy is not None:
            copy.wait_recv()

    def send_back(u, source, dest, sems):
        for r in sums[u]:
            for j in run_of(r):
                if j == 0:
                    dest[block(ep)] = source[block(ep)]
                else:
                    to = member(j)
                    send(
                        remote(
                            source.at[block(to)],
                            dest.at[block(ep)],
                            sems,
                            j,
                            (to, tp),
                            seen_as(j),
                        )
                    )

    def add_near(u):
        span = span_of(sums[u])
        part_wait(u, 0)
        part_sum[span] = (part[2, span].astype(F32) + part_in[0, span].astype(F32)).astype(BF16)
        if u >= 4:
            part_far_copies[u] = remote(
                part_sum.at[span], part_far.at[span], part_far_sem, u, (ep, far)
            )
            send(part_far_copies[u])
        else:
            send_back(u, part_sum, back_far, back_far_sem)

    def add_own(u):
        span = span_of(sums[u])
        part_wait(u, 1)
        final[span] = (part[3, span].astype(F32) + part_in[1, span].astype(F32)).astype(BF16)
        send_back(u, final, back, back_sem)

    def add_far(u):
        span = span_of(sums[u])
        part_wait(u, 1)
        near_sum = part[3, span].astype(F32) + part_in[1, span].astype(F32)
        part_far_copies[u].wait_recv()
        final[span] = (near_sum + part_far[span].astype(F32)).astype(BF16)
        send_back(u, final, back, back_sem)

    total_copy = remote(total_out, total_in, cross_sem, 1, (ep, far))
    begun = set()

    def add_rows(into, span, got):
        now = sum(
            lax.dot_general(
                table[span], got[span], (((0,), (0,)), ((), ())), preferred_element_type=F32
            )
            for table in (at_high, at_low)
        )
        if id(into) in begun:
            into[...] += now
        else:
            into[...] = now
        begun.add(id(into))

    def collect(u):
        span = span_of(sums[u])
        for r in sums[u]:
            for j in run_of(r):
                if j:
                    landed(back, back_sem, j)
        add_rows(total, span, back)

    def collect_far(u):
        span = span_of(sums[u])
        for r in sums[u]:
            for j in run_of(r):
                if j:
                    landed(back_far, back_far_sem, j)
        add_rows(total_far, span, back_far)

    def swap_totals():
        total_out[...] = total_far[...].astype(BF16)
        send(total_copy)

    def finish():
        total_copy.wait_recv()
        routed[...] = (total[...] + total_in[...].astype(F32)).astype(BF16)
        for copy in started:
            copy.wait_send()

    part_rows = length // n_tp

    def part_of(p):
        return pl.ds(pl.multiple_of(p * part_rows, 16), part_rows)

    share_copies = []

    def gate_rows(first, count):
        conv = jnp.zeros((count, chans), F32)
        for j in range(reach + 1):
            start = 16 - reach + j + first
            conv = conv + taps[j : j + 1, :] * prod[start : start + count, :]
        return (bgate[first : first + count, :].astype(F32) * conv).astype(BF16)

    def mix():
        wait_all(mix_loads[2:])
        prod[0:16, :] = jnp.zeros((16, chans), F32)
        prod[16:, :] = cgate[...].astype(F32) * inputs[...].astype(F32)
        gated[...] = gate_rows(0, length)

        def tile(i, carry):
            columns = pl.ds(pl.multiple_of(i * 256, 256), 256)
            share[:, columns] = dot(gated[...], wo[:, columns]).astype(BF16)
            return carry

        lax.fori_loop(0, d_all // 256, tile, 0, unroll=True)

    def mix_first():
        for copy in halo_copies:
            copy.wait_recv()
        before = halo[0].astype(F32) * halo[1].astype(F32)
        prod[0:16, :] = jnp.where(ep > 0, before, 0.0)
        share[0:16, :] = dot(gate_rows(0, 16), wo[...]).astype(BF16)
        for k in range(2):
            share_copies.append(
                remote(share.at[part_of(order[k])], share_in.at[k], share_sem, k, (ep, near))
            )
            send(share_copies[k])

    def mix_near(q):
        if q == 0:
            share_copies[0].wait_recv()
        columns = pl.ds(q * d, d)
        share_sum[:, columns] = (
            share[part_of(far), columns].astype(F32) + share_in[0, :, columns].astype(F32)
        ).astype(BF16)
        share_copies.append(
            remote(
                share_sum.at[:, columns], share_far.at[:, columns], share_sem, 2 + q, (ep, far)
            )
        )
        send(share_copies[2 + q])

    def mix_far():
        share_copies[1].wait_recv()
        near_sum = share[part_of(tp), :].astype(F32) + share_in[1].astype(F32)
        for q in range(4):
            share_copies[2 + q].wait_recv()
        mixed[...] = (near_sum + share_far[...].astype(F32)).astype(BF16)

    def tables():
        wait_all(late_loads)
        for unit in units.values():
            at = slots_of(unit)
            value = jnp.where(at == lane_slots[0], weight_t[0:1, :], 0.0) + jnp.where(
                at == lane_slots[1], weight_t[1:2, :], 0.0
            )
            span = span_of(unit)
            at_high[span], at_low[span] = split_terms(value)

    tiles = ff // 128
    loads = []

    def load_weights():
        for i in range(tiles):
            columns = pl.ds(i * 128, 128)
            for source, sem, at in ((w_gate, gate_sem, 0), (w_up, up_sem, 128)):
                loads.append(
                    pltpu.make_async_copy(
                        source.at[0, :, columns], wgu.at[:, pl.ds(i * 256 + at, 128)], sem.at[i]
                    )
                )
        loads.append(pltpu.make_async_copy(w_down.at[0], wd, plain_sem.at[0]))
        for copy in loads:
            copy.start()

    def load_wait():
        wait_all(loads)

    steps = {
        "D": depart,
        "P": pick_far,
        "G": depart_far,
        "A": arrive,
        "B": arrive_far,
        "R": relay,
        "C": compute,
        "O": compute_down,
        "N": add_near,
        "F": add_far,
        "H": add_own,
        "K": collect,
        "M": collect_far,
        "W": swap_totals,
        "X": mix,
        "Q": mix_first,
        "Y": mix_near,
        "Z": mix_far,
        "T": tables,
        "S": load_weights,
        "L": load_wait,
        "E": finish,
    }
    for step in PLAN:
        with scope(step):
            steps[step[0]](*(int(c) for c in step[1:]))


def publish(mixed, routed, mixed_out, routed_out, sems):
    copies = [
        pltpu.make_async_copy(mixed, mixed_out, sems.at[0]),
        pltpu.make_async_copy(routed, routed_out, sems.at[1]),
    ]
    for copy in copies:
        copy.start()
    for copy in copies:
        copy.wait()


def body(
    mix_bgate,
    mix_cgate,
    mix_input,
    conv_taps,
    mix_out_w,
    moe_x,
    moe_gain,
    routes,
    route_w,
    w_gate,
    w_up,
    w_down,
):
    ntok, d = moe_x.shape
    length, chans = mix_input.shape
    n_ep = lax.axis_size("ep")
    n_tp = lax.axis_size("tp")
    assert w_gate.shape[0] == 1 and n_tp == 4 and routes.shape[1] == 2
    assert n_ep & (n_ep - 1) == 0
    cap = sizes_of(ntok, routes.shape[1], n_ep)
    assert n_ep % 8 == 0
    wide_rows = n_ep // 4 * cap
    d_all = n_tp * d
    ff = w_down.shape[1]
    slots = n_ep * cap
    part_rows = length // n_tp
    vmem = pl.BlockSpec(memory_space=pltpu.VMEM)
    anywhere = pl.BlockSpec(memory_space=pl.ANY)
    dma = pltpu.SemaphoreType.DMA
    call = pl.pallas_call(
        functools.partial(kernel, n_ep, n_tp, cap),
        out_shape=(
            pltpu.VMEM((part_rows, d_all), BF16),
            pltpu.VMEM((ntok, d), BF16),
        ),
        in_specs=[anywhere] * 12,
        out_specs=(vmem, vmem),
        scratch_shapes=[
            pltpu.VMEM((ntok, d), BF16),
            pltpu.VMEM((2, ntok), jnp.int32),
            pltpu.VMEM((length, chans), BF16),
            pltpu.VMEM((length, chans), BF16),
            pltpu.VMEM((length, chans), BF16),
            pltpu.VMEM(conv_taps.shape, F32),
            pltpu.VMEM((2, ntok), F32),
            pltpu.VMEM((1, d_all), F32),
            pltpu.VMEM((d_all, 2 * ff), BF16),
            pltpu.VMEM((ff, d_all), BF16),
            pltpu.VMEM((chans, d_all), BF16),
            pltpu.VMEM((2, 16, chans), BF16),
            pltpu.VMEM((16 + length, chans), F32),
            pltpu.VMEM((length, chans), BF16),
            pltpu.VMEM((length, d_all), BF16),
            pltpu.VMEM((2, part_rows, d_all), BF16),
            pltpu.VMEM((part_rows, d_all), BF16),
            pltpu.VMEM((part_rows, d_all), BF16),
            pltpu.VMEM((ntok, d), BF16),
            pltpu.VMEM((slots, d), BF16),
            pltpu.VMEM((slots, d), BF16),
            pltpu.VMEM((slots, d_all), BF16),
            pltpu.VMEM((wide_rows, d_all), BF16),
            pltpu.VMEM((wide_rows, ff), BF16),
            pltpu.VMEM((4, slots, d), BF16),
            pltpu.VMEM((2, slots, d), BF16),
            pltpu.VMEM((slots, d), BF16),
            pltpu.VMEM((slots, d), BF16),
            pltpu.VMEM((slots, d), BF16),
            pltpu.VMEM((slots, d), BF16),
            pltpu.VMEM((slots, d), BF16),
            pltpu.VMEM((slots, ntok), BF16),
            pltpu.VMEM((slots, ntok), BF16),
            pltpu.VMEM((ntok, d), F32),
            pltpu.VMEM((ntok, d), F32),
            pltpu.VMEM((ntok, d), BF16),
            pltpu.VMEM((ntok, d), BF16),
            dma((9,)),
            dma((ff // 128,)),
            dma((ff // 128,)),
            dma((1,)),
            dma((2, 2)),
            dma((2, 6)),
            dma((2, 2)),
            dma((2, n_ep)),
            dma((2, n_ep)),
            dma((2, n_ep)),
            dma((2, n_ep)),
            dma((2, n_ep)),
            dma((2, 16)),
            dma((2, 8)),
            dma((2, n_ep)),
            dma((2, n_ep)),
        ],
        compiler_params=pltpu.CompilerParams(
            collective_id=0, has_side_effects=True, vmem_limit_bytes=56 << 20
        ),
        name="step",
    )
    results = call(
        mix_bgate,
        mix_cgate,
        mix_input,
        conv_taps,
        mix_out_w,
        moe_x,
        moe_gain.reshape(1, d_all),
        routes.T,
        route_w.T,
        w_gate,
        w_up,
        w_down,
    )
    return pl.pallas_call(
        publish,
        out_shape=(
            jax.ShapeDtypeStruct((part_rows, d_all), BF16),
            jax.ShapeDtypeStruct((ntok, d), BF16),
        ),
        in_specs=[vmem, vmem],
        out_specs=(anywhere, anywhere),
        scratch_shapes=[dma((2,))],
        compiler_params=pltpu.CompilerParams(vmem_limit_bytes=1 << 20),
        name="publish",
    )(*results)


def solution(mesh):
    in_specs = (
        P("ep", "tp"),
        P("ep", "tp"),
        P("ep", "tp"),
        P(None, "tp"),
        P("tp", None),
        P("ep", "tp"),
        P(),
        P("ep", None),
        P("ep", None),
        P("ep", None, "tp"),
        P("ep", None, "tp"),
        P("ep", "tp", None),
    )
    out_specs = (P(("ep", "tp"), None), P("ep", "tp"))
    return jax.shard_map(body, mesh=mesh, in_specs=in_specs, out_specs=out_specs, check_vma=False)
```

time: 76.2 us -> 54.3 us (0.71)
  the two profiles are of different devices: /device:TPU:21 before, /device:TPU:0 now
where the time goes in v1:
time: 54.3 us; the launch traced here: 54.2 us
  Pallas kernels  53.4 us (98%)
  between operations  0.8 us (1%)
    pallas_call x1, Pallas kernels, body(): call(mix_bgate, mix_cgate, mix_input, conv_taps, mix_out_w, moe_x, moe_ga...  52.6 us

profile of v1, /device:TPU:0, one launch (start us, length us, event | category | flops | bytes accessed | tf_op | source)
XLA Modules:
  0.0 54.2 jit_solution(9258897214830040821)
XLA Ops:
  0.6 52.6 %step.1 = (bf16[64,2048]{1,0:T(8,128)(2,1)S(1)}, bf16[256,512]{1,0:T(8,128)(2,1)S(1)}) custom-call(bf16[256,256]{1,0:T(8,128)(2,1)} %bgate_in.1, bf16[256,256]{1,0:T(8,128)(2,1)} %cgate_in.1, bf16[256,256]{1,0:T(8,128)(2,1)} %inputs_in.1, f32[3,256]{1,0:T(4,128)} %taps_in.1, bf16[256,2048]{1,0:T(8,128)(2,1)} %out_w.1, bf16[256,512]{1,0:T(8,128)(2,1)} %x_in.1, ...), custom_call_target="tpu_custom_call" | custom-call | tf_op jit(solution)/shard_map/step/pallas_call | solution.py:673
  53.2 0.8 %publish.1 = (bf16[64,2048]{1,0:T(8,128)(2,1)}, bf16[256,512]{1,0:T(8,128)(2,1)}) custom-call(bf16[64,2048]{1,0:T(8,128)(2,1)S(1)} %get-tuple-element.4.mixed, bf16[256,512]{1,0:T(8,128)(2,1)S(1)} %get-tuple-element.5.routed), custom_call_target="tpu_custom_call" | custom-call | tf_op jit(solution)/shard_map/publish/pallas_call | solution.py:687

commit v2 on v1

--- a/solution.py
+++ b/solution.py
@@ -13,11 +13,11 @@
 scope = jax.named_scope
 
 PLAN = (
-    "D4", "D6", "D1", "D2", "D3", "A0", "S", "X", "T", "A1", "Q", "A4", "P", "G2", "G1", "D5",
-    "G3", "D7", "B0", "Y0", "A2", "R4", "A6", "Y1", "L", "C4", "A3", "B2", "O4", "R6", "C0",
-    "N4", "A5", "O0", "Y2", "B1", "B3", "C6", "F4", "O6", "A7", "N0", "N6", "C1", "R5", "O1",
-    "Y3", "N1", "C5", "F6", "R7", "O5", "H0", "N5", "C7", "H1", "O7", "M0", "N7", "F5", "M1",
-    "W", "F7", "Z", "K4", "K0", "K6", "K1", "K5", "K7", "E",
+    "D6", "D4", "I", "D1", "D2", "D3", "A0", "S", "X", "T", "A1", "Q", "Y0", "A4", "P", "G2",
+    "G1", "D7", "G3", "D5", "B0", "A2", "R4", "A6", "Y1", "L", "C4", "A3", "B2", "O4", "R6",
+    "C0", "N4", "O0", "A5", "B1", "B3", "C6", "A7", "O6", "F4", "N6", "N0", "C1", "R5", "Y2",
+    "O1", "Y3", "N1", "R7", "C5", "F6", "O5", "H0", "N5", "C7", "H1", "O7", "M0", "N7", "F5",
+    "M1", "W", "F7", "Z", "K4", "K0", "K6", "K1", "K5", "K7", "E",
 )
 
 
@@ -219,10 +219,10 @@
         hit = (at == lane_slots[0]) | (at == lane_slots[1])
         return jnp.where(hit, 1.0, 0.0).astype(BF16)
 
-    for unit in ((0, 2), (1, 3), (4, 6), (5, 7)):
+    def pick(unit):
         sent[span_of(unit)] = dot(hits(unit), x[...]).astype(BF16)
-    rows[block(ep), mine] = sent[block(ep)]
-
+
+    pick((4, 6))
     with scope("barrier"):
         pl.semaphore_wait(barrier, n_ep + 1)
 
@@ -269,6 +269,11 @@
 
     go = {j: go_copy(j) for j in range(1, n_ep)}
     go_far = {j: go_far_copy(j) for j in range(1, n_ep // 2)}
+
+    def pick_rest():
+        for unit in ((0, 2), (1, 3), (5, 7)):
+            pick(unit)
+        rows[block(ep), mine] = sent[block(ep)]
 
     def depart(r):
         for j in run_of(r):
@@ -534,6 +539,7 @@
 
     steps = {
         "D": depart,
+        "I": pick_rest,
         "P": pick_far,
         "G": depart_far,
         "A": arrive,

time: 54.3 us -> 54.1 us (level)
  no operation moved by 1% of the time
where the time goes in v2:
time: 54.1 us; the launch traced here: 53.7 us
  Pallas kernels  52.9 us (98%)
  between operations  0.8 us (1%)
    pallas_call x1, Pallas kernels, body(): call(mix_bgate, mix_cgate, mix_input, conv_taps, mix_out_w, moe_x, moe_ga...  52.1 us

profile of v2, /device:TPU:0, one launch (start us, length us, event | category | flops | bytes accessed | tf_op | source)
XLA Modules:
  0.0 53.7 jit_solution(1359032969047170540)
XLA Ops:
  0.6 52.1 %step.1 = (bf16[64,2048]{1,0:T(8,128)(2,1)S(1)}, bf16[256,512]{1,0:T(8,128)(2,1)S(1)}) custom-call(bf16[256,256]{1,0:T(8,128)(2,1)} %bgate_in.1, bf16[256,256]{1,0:T(8,128)(2,1)} %cgate_in.1, bf16[256,256]{1,0:T(8,128)(2,1)} %inputs_in.1, f32[3,256]{1,0:T(4,128)} %taps_in.1, bf16[256,2048]{1,0:T(8,128)(2,1)} %out_w.1, bf16[256,512]{1,0:T(8,128)(2,1)} %x_in.1, ...), custom_call_target="tpu_custom_call" | custom-call | tf_op jit(solution)/shard_map/step/pallas_call | solution.py:679
  52.7 0.8 %publish.1 = (bf16[64,2048]{1,0:T(8,128)(2,1)}, bf16[256,512]{1,0:T(8,128)(2,1)}) custom-call(bf16[64,2048]{1,0:T(8,128)(2,1)S(1)} %get-tuple-element.4.mixed, bf16[256,512]{1,0:T(8,128)(2,1)S(1)} %get-tuple-element.5.routed), custom_call_target="tpu_custom_call" | custom-call | tf_op jit(solution)/shard_map/publish/pallas_call | solution.py:693
